TPU v7x, 32 devices: a whole 2x2x4 slice. The times are simulated.
32 devices in a mesh: dp: 4 (over y, x), kv: 4 (over z), tp: 2 (over core).
Axes of the slice: x: 2, y: 2, z: 4, core: 2. Of those that a mesh axis runs over, the one named last changes fastest.
Arguments:
- tokens: bfloat16 [2048, 2048], P('dp', 'kv'), may hold values from -70 to 70
- pre_gain: float32 [2048], replicated, may hold values from 0.1 to 1.9
- query_weight: bfloat16 [2048, 1024], P(None, 'tp'), may hold values from -0.125 to 0.125
- key_weight: bfloat16 [2048, 1024], P(None, 'tp'), may hold values from -0.125 to 0.125
- value_weight: bfloat16 [2048, 1024], P(None, 'tp'), may hold values from -0.125 to 0.125
- gate_weight: bfloat16 [2048, 1024], P(None, 'tp'), may hold values from -0.125 to 0.125
- beta_weight: bfloat16 [2048, 8], replicated, may hold values from -0.125 to 0.125
- decay_weight: bfloat16 [2048, 8], replicated, may hold values from -0.125 to 0.125
- decay_log: float32 [8], P('tp'), may hold values from -3 to 0.5
- head_gain: float32 [128], replicated, may hold values from 0.1 to 1.9
- out_weight: bfloat16 [1024, 2048], P('tp', 'kv'), may hold values from -1 to 1
- post_gain: float32 [2048], P(('kv', 'tp')), may hold values from 0.1 to 1.9
- saved_state: float32 [512, 8, 128, 128], P(('dp', 'kv'), 'tp'), may hold values from -4 to 4
- earlier_keys: bfloat16 [512, 4, 8, 128], P(('dp', 'kv'), None, 'tp'), may hold values from -6 to 6
- earlier_values: bfloat16 [512, 4, 8, 128], P(('dp', 'kv'), None, 'tp'), may hold values from -6 to 6
- earlier_rates: float32 [512, 4, 8], P(('dp', 'kv'), None, 'tp'), may hold values from 0.05 to 0.95
- earlier_decays: float32 [512, 4, 8], P(('dp', 'kv'), None, 'tp'), may hold values from -1.5 to -0.02
- accepted: int32 [512], P(('dp', 'kv')), may hold values from 0 to 4
Outputs:
- mixed: bfloat16 [2048, 2048], P('dp', ('kv', 'tp'))
- committed: float32 [512, 8, 128, 128], P(('dp', 'kv'), 'tp')
All inputs are finite; a program needn't handle non-finite values.
Results may differ from a plain program's by a relative error of at most 0.011.
Values may be sent and summed in bfloat16 or wider, within the bound.
A program may use at most 128 MiB of HBM per device.

v0:
```python
import jax
import jax.numpy as jnp
from jax import lax
from jax.sharding import PartitionSpec as P


def unit_norm(values):
    return values * lax.rsqrt(jnp.sum(values * values, axis=-1, keepdims=True) + 1e-06)


def advance(current, key_row, value_row, rate_now, log_decay):
    recalled = jnp.sum(key_row[..., :, None] * current, axis=-2)
    rate_cube = rate_now[..., None, None]
    current = current - rate_cube * key_row[..., :, None] * recalled[..., None, :]
    return (
        jnp.exp(log_decay)[..., None, None] * current
        + rate_cube * key_row[..., :, None] * value_row[..., None, :]
    )


def run_heads(
    saved_state,
    earlier_keys,
    earlier_values,
    earlier_rates,
    earlier_decays,
    accepted,
    queries,
    keys_unit,
    values_act,
    rates,
    decays,
):
    current = saved_state
    proposals = earlier_keys.shape[1]
    for position in range(proposals):
        live = (position < accepted).astype(jnp.float32)
        live = live.reshape(live.shape + (1,) * (earlier_rates.ndim - 2))
        current = advance(
            current,
            earlier_keys[:, position],
            earlier_values[:, position],
            earlier_rates[:, position] * live,
            earlier_decays[:, position] * live,
        )
    committed = current
    outputs = []
    for position in range(proposals):
        current = advance(
            current,
            keys_unit[:, position],
            values_act[:, position],
            rates[:, position],
            decays[:, position],
        )
        outputs.append(jnp.sum(queries[:, position][..., :, None] * current, axis=-2))
    return (committed, jnp.stack(outputs, axis=1))


def local(
    tokens,
    pre_gain,
    query_weight,
    key_weight,
    value_weight,
    gate_weight,
    beta_weight,
    decay_weight,
    decay_log,
    head_gain,
    out_weight,
    post_gain,
    saved_state,
    earlier_keys,
    earlier_values,
    earlier_rates,
    earlier_decays,
    accepted,
):
    seq_local = saved_state.shape[0]
    heads_local = saved_state.shape[1]
    head_size = saved_state.shape[2]
    proposals = earlier_keys.shape[1]
    rows_local = seq_local * proposals
    width_local = heads_local * head_size
    model_width = pre_gain.shape[0]
    head_start = lax.axis_index("tp") * heads_local
    beta_cols = lax.dynamic_slice_in_dim(beta_weight, head_start, heads_local, 1)
    decay_cols = lax.dynamic_slice_in_dim(decay_weight, head_start, heads_local, 1)
    own_rows = lax.all_to_all(tokens, "kv", split_axis=0, concat_axis=1, tiled=True)
    widened = own_rows.astype(jnp.float32)
    inverse = lax.rsqrt(jnp.mean(widened * widened, axis=1) + 1e-06)
    scaled = (widened * pre_gain).astype(jnp.bfloat16)
    stacked = jnp.stack(
        [
            jnp.dot(scaled, weight, preferred_element_type=jnp.float32)
            for weight in (query_weight, key_weight, value_weight, gate_weight)
        ],
        axis=1,
    )
    scalars = jnp.stack(
        [
            jnp.dot(scaled, cols, preferred_element_type=jnp.float32)
            for cols in (beta_cols, decay_cols)
        ],
        axis=1,
    )
    stacked = stacked * inverse[:, None, None]
    scalars = scalars * inverse[:, None, None]

    def heads_of(values):
        return values.reshape(seq_local, proposals, heads_local, head_size)

    queries = unit_norm(jax.nn.silu(heads_of(stacked[:, 0]))) * head_size ** (-0.5)
    keys_unit = unit_norm(jax.nn.silu(heads_of(stacked[:, 1])))
    values_act = jax.nn.silu(heads_of(stacked[:, 2]))
    gates_raw = heads_of(stacked[:, 3])
    rates = jax.nn.sigmoid(scalars[:, 0]).reshape(seq_local, proposals, heads_local)
    decays = -jnp.exp(decay_log) * jax.nn.softplus(scalars[:, 1]).reshape(
        seq_local, proposals, heads_local
    )
    committed, reads = run_heads(
        saved_state,
        unit_norm(earlier_keys.astype(jnp.float32)),
        earlier_values.astype(jnp.float32),
        earlier_rates,
        earlier_decays,
        accepted,
        queries,
        keys_unit,
        values_act,
        rates,
        decays,
    )
    normed = reads * lax.rsqrt(jnp.mean(reads * reads, axis=-1, keepdims=True) + 1e-06) * head_gain
    attended = (
        (normed * jax.nn.silu(gates_raw)).reshape(rows_local, width_local).astype(jnp.bfloat16)
    )
    partial_value = jnp.dot(
        lax.all_gather(attended, "kv", axis=0, tiled=True),
        out_weight,
        preferred_element_type=jnp.float32,
    )
    column_part = lax.psum_scatter(
        partial_value.astype(jnp.bfloat16), "tp", scatter_dimension=1, tiled=True
    ).astype(jnp.float32)
    totals = lax.psum(jnp.sum(column_part * column_part, axis=1), ("kv", "tp"))
    factor = lax.rsqrt(totals / model_width + 1e-06)
    mixed = (column_part * factor[:, None] * post_gain).astype(jnp.bfloat16)
    return (mixed, committed)


def solution(mesh):
    placed = (
        P("dp", "kv"),
        P(),
        P(None, "tp"),
        P(None, "tp"),
        P(None, "tp"),
        P(None, "tp"),
        P(),
        P(),
        P("tp"),
        P(),
        P("tp", "kv"),
        P(("kv", "tp")),
        P(("dp", "kv"), "tp", None, None),
        P(("dp", "kv"), None, "tp", None),
        P(("dp", "kv"), None, "tp", None),
        P(("dp", "kv"), None, "tp"),
        P(("dp", "kv"), None, "tp"),
        P(("dp", "kv")),
    )
    return jax.shard_map(
        local,
        mesh=mesh,
        in_specs=placed,
        out_specs=(P("dp", ("kv", "tp")), P(("dp", "kv"), "tp", None, None)),
        check_vma=False,
    )
```

profile of v0, /device:TPU:0, one launch (start us, length us, event | category | flops | bytes accessed | tf_op | source)
XLA Modules:
  0.0 188.2 jit_solution(8229419041225215411)
XLA Ops:
  7.2 6.5 %all-to-all-start = ((bf16[4,128,512]{2,1,0:T(8,128)(2,1)}), bf16[4,128,512]{2,1,0:T(8,128)(2,1)S(1)}, u32[]{:S(2)}, u32[]{:S(2)}) async-start(bf16[4,128,512]{2,1,0:T(8,128)(2,1)} %bitcast.148), calls=%async_computation | async-start | bytes 1048576 | tf_op jit(solution)/shard_map/all_to_all | solution.py:90
  13.7 1.2 broadcast_bitcast_fusion
  14.9 0.7 compare_convert_fusion.3
  15.6 0.8 bitcast_multiply_fusion.2
  17.0 1.1 fusion.43
  18.2 1.1 convert_multiply_fusion.3
  19.3 0.9 convert_element_type.56
  20.5 9.6 %multiply_add_fusion.6 = f32[32,4,128,128]{3,2,1,0:T(8,128)S(1)} fusion(f32[32,4,128,128]{3,2,1,0:T(8,128)} %param.30, f32[32,4,128]{2,1,0:T(4,128)S(1)} %get-tuple-element.34, f32[32,4,128]{2,1,0:T(4,128)S(1)} %get-tuple-element.30, f32[32,4]{1,0:T(8,128)S(1)} %copy.66, f32[32,4,128]{2,1,0:T(4,128)S(1)} %get-tuple-element.65), kind=kOutput, calls=%fused_computation.32 | output fusion | flops 12599423 | bytes 16974336 | tf_op jit(solution)/shard_map/mul | solution.py:14
  30.1 15.4 %multiply_add_fusion.5 = f32[32,4,128,128]{3,2,1,0:T(8,128)S(1)} fusion(f32[32,4,128,128]{3,2,1,0:T(8,128)S(1)} %multiply_add_fusion.6, f32[32,4,128]{2,1,0:T(4,128)S(1)} %get-tuple-element.33, f32[32,4,128]{2,1,0:T(4,128)S(1)} %get-tuple-element.29, f32[32,4]{1,0:T(8,128)S(1)} %copy.65, f32[32,4,128]{2,1,0:T(4,128)S(1)} %get-tuple-element.66), kind=kOutput, calls=%fused_computation.29 | output fusion | flops 12599423 | bytes 16974336 | tf_op jit(solution)/shard_map/mul | solution.py:14
  45.6 7.2 %multiply_add_fusion.4 = f32[32,4,128,128]{3,2,1,0:T(8,128)} fusion(f32[32,4,128,128]{3,2,1,0:T(8,128)S(1)} %multiply_add_fusion.5, f32[32,4,128]{2,1,0:T(4,128)S(1)} %get-tuple-element.32, f32[32,4,128]{2,1,0:T(4,128)S(1)} %get-tuple-element.28, f32[32,4]{1,0:T(8,128)S(1)} %copy.64, f32[32,4,128]{2,1,0:T(4,128)S(1)} %get-tuple-element.67), kind=kOutput, calls=%fused_computation.26 | output fusion | flops 12599423 | bytes 16974336 | tf_op jit(solution)/shard_map/mul | solution.py:14
  52.9 12.1 %multiply_add_fusion.3 = f32[32,4,128,128]{3,2,1,0:T(8,128)} fusion(f32[32,4,128,128]{3,2,1,0:T(8,128)} %multiply_add_fusion.4, f32[32,4,128]{2,1,0:T(4,128)S(1)} %get-tuple-element.31, f32[32,4,128]{2,1,0:T(4,128)S(1)} %get-tuple-element.27, f32[32,4]{1,0:T(8,128)S(1)} %copy.63, f32[32,4,128]{2,1,0:T(4,128)S(1)} %get-tuple-element.68), kind=kOutput, calls=%fused_computation.23 | output fusion | flops 12599423 | bytes 16974336 | tf_op jit(solution)/shard_map/mul | solution.py:14
  65.2 1.1 convert_bitcast_fusion
  66.3 2.6 %copy.61 = f32[128,4,512]{0,2,1:T(8,128)} copy(f32[128,4,512]{2,0,1:T(8,128)} %convert_bitcast_fusion) | data formatting | bytes 2097152 | tf_op jit(solution)/shard_map/convert_element_type | solution.py:91
  68.9 1.6 fusion.39
  73.0 0.9 copy.82
  73.9 0.9 copy.80
  74.8 0.9 copy.78
  75.6 0.5 convolution_bitcast_fusion
  76.1 2.2 %convolution_bitcast_fusion.1 = f32[128,1,512]{2,0,1:T(8,128)S(1)} fusion(bf16[128,2048]{0,1:T(8,128)(2,1)S(1)} %fusion.39, bf16[2048,512]{1,0:T(8,128)(2,1)} %param.22), kind=kOutput, calls=%fused_computation.47 | convolution fusion | flops 268435456 | bytes 2883584 | tf_op jit(solution)/shard_map/dot_general | solution.py:96
  78.3 2.1 %convolution_bitcast_fusion.2 = f32[128,1,512]{2,0,1:T(8,128)S(1)} fusion(bf16[128,2048]{0,1:T(8,128)(2,1)S(1)} %fusion.39, bf16[2048,512]{1,0:T(8,128)(2,1)} %param.21), kind=kOutput, calls=%fused_computation.48 | convolution fusion | flops 268435456 | bytes 2883584 | tf_op jit(solution)/shard_map/dot_general | solution.py:96
  80.4 0.5 convolution_bitcast_fusion.3
  81.7 0.7 slice_bitcast_fusion.20
  83.6 12.4 %multiply_reduce_fusion.6 = (f32[32,4,128]{2,1,0:T(4,128)S(1)}, f32[32,4,128,128]{3,2,1,0:T(8,128)S(1)}) fusion(f32[32,4,128]{2,1,0:T(4,128)S(1)} %get-tuple-element.7, f32[32,4,128]{2,1,0:T(4,128)S(1)} %get-tuple-element.22, f32[32,4,128,128]{3,2,1,0:T(8,128)} %multiply_add_fusion.3, f32[32,4,128]{2,1,0:T(4,128)S(1)} %get-tuple-element.69, ...), kind=kOutput, calls=%fused_computation.19 | output fusion | flops 16777344 | bytes 17105408 | tf_op jit(solution)/shard_map/mul | solution.py:14
  96.1 9.0 %multiply_reduce_fusion.4 = (f32[32,4,128]{2,1,0:T(4,128)S(1)}, f32[32,4,128,128]{3,2,1,0:T(8,128)}) fusion(f32[32,4,128]{2,1,0:T(4,128)S(1)} %get-tuple-element.10, f32[32,4,128]{2,1,0:T(4,128)S(1)} %get-tuple-element.21, f32[32,4,128,128]{3,2,1,0:T(8,128)S(1)} %get-tuple-element.64, f32[32,4,128]{2,1,0:T(4,128)S(1)} %get-tuple-element.70, ...), kind=kOutput, calls=%fused_computation.15 | output fusion | flops 16777344 | bytes 17105408 | tf_op jit(solution)/shard_map/mul | solution.py:14
  105.1 14.0 %fusion = f32[32,4,128,128]{3,2,1,0:T(8,128)} fusion(f32[32,4,128]{2,1,0:T(4,128)S(1)} %get-tuple-element.72, f32[32,4,128,128]{3,2,1,0:T(8,128)} %get-tuple-element.62, f32[32,4,128]{2,1,0:T(4,128)S(1)} %get-tuple-element.20, f32[32,4,128]{2,1,0:T(4,128)S(1)} %get-tuple-element.12, f32[32,4]{1,0:T(8,128)S(1)} %bitcast.163, ...), kind=kOutput, calls=%fused_computation | output fusion | flops 14713086 | bytes 17039872 | tf_op jit(solution)/shard_map/mul | solution.py:14
  119.1 14.9 %multiply_reduce_fusion.2 = (f32[32,4,128]{2,1,0:T(4,128)S(1)}, f32[32,4,128]{2,1,0:T(4,128)S(1)}) fusion(f32[32,4,128]{2,1,0:T(4,128)} %get-tuple-element.9, f32[32,4,128]{2,1,0:T(4,128)S(1)} %get-tuple-element.19, f32[32,4,128,128]{3,2,1,0:T(8,128)} %fusion, f32[32,4,128]{2,1,0:T(4,128)S(1)} %get-tuple-element.11, f32[32,4]{1,0:T(8,128)S(1)} %bitcast.161, ...), kind=kOutput, calls=%fused_computation.11 | output fusion | flops 31441024 | bytes 17368064 | tf_op jit(solution)/shard_map/mul | solution.py:14
  134.6 15.7 %all_gather.3 = bf16[512,512]{1,0:T(8,128)(2,1)S(1)} all-gather(bf16[128,512]{1,0:T(8,128)(2,1)S(1)} %fusion.45), channel_id=1, replica_groups=mesh['dp'=4,'kv'=4,'tp'=2] {'kv'}, dimensions={0}, use_global_device_ids=true | all-gather | bytes 655360 | tf_op jit(solution)/shard_map/all_gather | solution.py:140
  150.3 1.2 convolution_convert_fusion
  151.6 9.8 %reduce-scatter.2.cloned.1.call-done = bf16[512,256]{1,0:T(8,128)(2,1)} async-done(((bf16[512,512]{1,0:T(8,128)(2,1)}), bf16[512,256]{1,0:T(8,128)(2,1)}) %reduce-scatter.2.cloned.1.call-update) | async-done | bytes 262160 | tf_op jit(solution)/shard_map/reduce_scatter | solution.py:144
  161.4 1.1 fusion.40
  162.5 17.1 %psum.7 = f32[512]{0:T(512)S(1)} all-reduce(f32[512]{0:T(512)S(1)} %fusion.40), channel_id=1, replica_groups=mesh['dp'=4,'kv'=4,'tp'=2] {'kv','tp'}, use_global_device_ids=true, to_apply=%region_19.20 | all-reduce | flops 512 | bytes 4096 | tf_op jit(solution)/shard_map/psum | solution.py:147
  179.6 1.8 fusion.42
  (76 shorter events, 6.3 us)
Async XLA Ops:
  7.2 68.5 %copy-start = (bf16[2048,512]{1,0:T(8,128)(2,1)S(1)}, bf16[2048,512]{1,0:T(8,128)(2,1)}, u32[]{:S(2)}) copy-start(bf16[2048,512]{1,0:T(8,128)(2,1)} %param.23) | copy-start | bytes 6291460
  7.2 57.8 %all-to-all-start = ((bf16[4,128,512]{2,1,0:T(8,128)(2,1)}), bf16[4,128,512]{2,1,0:T(8,128)(2,1)S(1)}, u32[]{:S(2)}, u32[]{:S(2)}) async-start(bf16[4,128,512]{2,1,0:T(8,128)(2,1)} %bitcast.148), calls=%async_computation | async-start | bytes 1048576 | tf_op jit(solution)/shard_map/all_to_all | solution.py:90
  13.7 147.7 %reduce-scatter.2.cloned.1.call-start = ((), (), s32[]{:S(2)}) async-start(), calls=%async_computation.2 | async-start | bytes 786432 | tf_op jit(solution)/shard_map/reduce_scatter | solution.py:144
  45.5 7.2 %copy-start.12 = (f32[4]{0:T(128)S(1)}, f32[4]{0:T(128)}, u32[]{:S(2)}) copy-start(f32[4]{0:T(128)} %param.26) | copy-start | bytes 52
  52.9 16.0 %copy-start.8 = (f32[2048]{0:T(1024)S(1)}, f32[2048]{0:T(1024)}, u32[]{:S(2)}) copy-start(f32[2048]{0:T(1024)} %param.19) | copy-start | bytes 24580
  52.9 17.6 %copy-start.10 = (bf16[2048,8]{0,1:T(8,128)(2,1)S(1)}, bf16[2048,8]{0,1:T(8,128)(2,1)}, u32[]{:S(2)}) copy-start(bf16[2048,8]{0,1:T(8,128)(2,1)} %param.25) | copy-start | bytes 98308
  52.9 17.8 %copy-start.11 = (bf16[2048,8]{0,1:T(8,128)(2,1)S(1)}, bf16[2048,8]{0,1:T(8,128)(2,1)}, u32[]{:S(2)}) copy-start(bf16[2048,8]{0,1:T(8,128)(2,1)} %param.24) | copy-start | bytes 98308
  75.6 4.8 %copy-start.2 = (bf16[2048,512]{1,0:T(8,128)(2,1)S(1)}, bf16[2048,512]{1,0:T(8,128)(2,1)}, u32[]{:S(2)}) copy-start(bf16[2048,512]{1,0:T(8,128)(2,1)} %param.20) | copy-start | bytes 6291460
  78.3 5.3 %copy-start.7 = (f32[32,1,4]{2,0,1:T(8,128)S(1)}, f32[32,1,4]{2,0,1:T(8,128)}, u32[]{:S(2)}) copy-start(f32[32,1,4]{2,0,1:T(8,128)} %copy.78) | copy-start | bytes 1540
  83.6 21.5 %copy-start.4 = (f32[32,4,128]{2,1,0:T(4,128)}, f32[32,4,128]{2,1,0:T(4,128)S(1)}, u32[]{:S(2)}) copy-start(f32[32,4,128]{2,1,0:T(4,128)S(1)} %get-tuple-element.12) | copy-start | bytes 196612
  83.6 12.5 %copy-start.6 = (f32[32,1,4]{2,0,1:T(8,128)S(1)}, f32[32,1,4]{2,0,1:T(8,128)}, u32[]{:S(2)}) copy-start(f32[32,1,4]{2,0,1:T(8,128)} %copy.80) | copy-start | bytes 1540
  96.1 9.0 %copy-start.5 = (f32[32,1,4]{2,0,1:T(8,128)S(1)}, f32[32,1,4]{2,0,1:T(8,128)}, u32[]{:S(2)}) copy-start(f32[32,1,4]{2,0,1:T(8,128)} %copy.82) | copy-start | bytes 1540
  119.1 15.4 %copy-start.9 = (f32[512]{0:T(512)S(1)}, f32[512]{0:T(512)}, u32[]{:S(2)}) copy-start(f32[512]{0:T(512)} %broadcast_bitcast_fusion) | copy-start | bytes 6148
  119.1 31.2 %copy-start.3 = (bf16[512,512]{1,0:T(8,128)(2,1)S(1)}, bf16[512,512]{1,0:T(8,128)(2,1)}, u32[]{:S(2)}) copy-start(bf16[512,512]{1,0:T(8,128)(2,1)} %param.28) | copy-start | bytes 1572868
  119.1 62.3 %copy-start.1 = (bf16[2048,512]{1,0:T(8,128)(2,1)S(1)}, bf16[2048,512]{1,0:T(8,128)(2,1)}, u32[]{:S(2)}) copy-start(bf16[2048,512]{1,0:T(8,128)(2,1)} %param.23) | copy-start | bytes 6291460
Sparse Core Ops, SparseCore 0:
  151.7 9.6 reduce-scatter.1
where the time goes:
time: 189 us; the launch traced here: 188 us
  other arithmetic  107 us (57%)
  blocking collectives  32.7 us (17%)
  between operations  14.4 us (8%)
  local copies, waits for them, and re-layouts  10.4 us (6%)
  waiting for transfers between devices  9.86 us (5%)
  matrix products  6.8 us (4%)
  starting transfers between devices  6.49 us (3%)
    mul x10, other arithmetic, advance(): rate_cube * key_row[..., :, None] * recalled[..., None, :]  95.1 us
    psum x1, blocking collectives, local(): totals = lax.psum(jnp.sum(column_part * column_part, axis=1), ('kv', 'tp'))  17.1 us
    all_gather x1, blocking collectives, local(): lax.all_gather(attended, 'kv', axis=0, tiled=True)  15.7 us
    reduce_scatter x1, waiting for transfers between devices, local(): lax.psum_scatter(partial_value.astype(jnp.bfloat16), 'tp', scatter_dimens...  9.84 us
    all_to_all x1, starting transfers between devices, local(): lax.all_to_all(tokens, 'kv', split_axis=0, concat_axis=1, tiled=True)  6.49 us
    dot_general x4, matrix products, local(): jnp.dot(scaled, weight, preferred_element_type=jnp.float32)  5.2 us
  transfers between devices with their start and end apart: 2, of which 1 were waited for; matrix products, arithmetic and copies ran while one was open for 27% of the time, Pallas kernels for 0%

commit v1 on v0

v1 whole, which is shorter than its diff:
```python
import functools

import jax
import jax.numpy as jnp
from jax import lax
from jax.experimental import pallas as pl
from jax.experimental.pallas import tpu as pltpu
from jax.sharding import PartitionSpec as P

F32 = jnp.float32
BF16 = jnp.bfloat16
EPS = 1e-06
MESH_IDS = pl.DeviceIdType.MESH
VMEM_BYTES = 60 * 1024 * 1024


def mm(a, b):
    return jnp.dot(a, b, preferred_element_type=F32)


def mm_nt(a, b):
    return lax.dot_general(a, b, (((1,), (1,)), ((), ())), preferred_element_type=F32)


def mm_tn(a, b):
    return lax.dot_general(a, b, (((0,), (0,)), ((), ())), preferred_element_type=F32)


def mm_exact(a, b):
    return jnp.dot(a, b, preferred_element_type=F32, precision=lax.Precision.HIGHEST)


def unit(values):
    return values * lax.rsqrt(jnp.sum(values * values, axis=-1, keepdims=True) + EPS)


def silu(values):
    return values / (1.0 + jnp.exp(-values))


def masks_of(rows, proposals):
    r = lax.broadcasted_iota(jnp.int32, (rows, rows), 0)
    c = lax.broadcasted_iota(jnp.int32, (rows, rows), 1)
    same = (r // proposals) == (c // proposals)
    return same, same & (c <= r), same & (c < r)


def per_sequence(operands, state_of, proposals, rows):
    size = operands[0].shape[1]
    group = 16
    seqs = group // proposals
    stack = group * len(operands)
    row = lax.broadcasted_iota(jnp.int32, (stack, size), 0)
    owner = (row % group) // proposals
    outs = [[] for _ in operands]
    for g in range(rows // group):
        x = jnp.concatenate([o[g * group:(g + 1) * group] for o in operands], axis=0)
        lhs = jnp.concatenate(
            [jnp.where(owner == s, x, 0.0).astype(BF16) for s in range(seqs)], axis=1
        )
        rhs = state_of(g * seqs, seqs).reshape(seqs * size, size).astype(BF16)
        y = mm(lhs, rhs)
        for i in range(len(operands)):
            outs[i].append(y[i * group:(i + 1) * group])
    return [jnp.concatenate(o, axis=0) for o in outs]


def solve(keys, values, recalled, rate, decay_pairs, gamma, strict):
    kb = keys.astype(BF16)
    low = (jnp.where(strict, decay_pairs * mm_nt(kb, kb), 0.0) * rate).astype(BF16)
    rhs = rate * (values - gamma * recalled)
    square = mm(low, low).astype(BF16)
    x = rhs + mm(square, rhs.astype(BF16))
    return x - mm(low, x.astype(BF16))


def commit_kernel(proposals, heads, keys_ref, values_ref, bg_ref, state_ref, out_ref, cum, cum_t, last):
    h = pl.program_id(0)
    rows, size = keys_ref.shape
    same, incl, strict = masks_of(rows, proposals)

    bg = bg_ref[...]
    total = mm_exact(jnp.where(incl, 1.0, 0.0), bg)
    cum[...] = total
    cum_t[...] = total.T
    last[...] = mm_exact(jnp.where(same, 1.0, 0.0), bg)
    lane = lax.broadcasted_iota(jnp.int32, (rows, rows), 1)

    def column(ref, j):
        return jnp.sum(jnp.where(lane == j, ref[...], 0.0), axis=1, keepdims=True)

    rate = column(bg_ref, h)
    g_col = column(cum, heads + h)
    g_last = column(last, heads + h)
    g_row = cum_t[pl.ds(heads + h, 1), :]
    pairs = jnp.exp(jnp.where(incl, g_col - g_row, -1e30))
    keys = unit(keys_ref[...].astype(F32))
    (recalled,) = per_sequence(
        [keys], lambda s, n: state_ref[s:s + n, 0], proposals, rows
    )
    w = solve(keys, values_ref[...].astype(F32), recalled, rate, pairs, jnp.exp(g_col), strict)
    scaled_keys = (keys * jnp.exp(g_last - g_col)).astype(BF16)
    whole = jnp.broadcast_to(jnp.exp(g_last), (rows, size))
    group = 16
    seqs = group // proposals
    owner = lax.broadcasted_iota(jnp.int32, (group, size), 0) // proposals
    for g in range(rows // group):
        wg = w[g * group:(g + 1) * group]
        spread = jnp.concatenate(
            [jnp.where(owner == s, wg, 0.0).astype(BF16) for s in range(seqs)], axis=1
        )
        add = mm_tn(scaled_keys[g * group:(g + 1) * group], spread)
        for s in range(seqs):
            seq = g * seqs + s
            keep = whole[seq * proposals:seq * proposals + 1]
            out_ref[seq, 0] = keep * state_ref[seq, 0] + add[:, s * size:(s + 1) * size]


def layer_kernel(
    kv, tp, proposals, heads, model_width,
    tokens, gains, qw, kw, vw, gw, bd, log_row, head_gain, ow, post, state,
    out,
    tok, wv, sv, owv, acc, sacc, att, attall, part, give, take, sums, sumall,
    w_sem, s_sem, ow_sem, own_sem, tok_send, tok_recv, att_send, att_recv, own_att,
    tp_send, tp_recv, sum_send, sum_recv,
):
    me = lax.axis_index("kv")
    core = lax.axis_index("tp")
    rows, chunk = tok.shape[1], tok.shape[2]
    size = head_gain.shape[1]
    cols = out.shape[1]
    weights = (qw, kw, vw, gw)

    def source(d):
        return lax.rem(me - d + kv, kv)

    def target(d):
        return lax.rem(me + d, kv)

    local = {}
    local["tok"] = pltpu.make_async_copy(tokens.at[pl.ds(me * rows, rows), :], tok.at[0], own_sem)
    local["tok"].start()
    for d in range(kv):
        for i in range(4):
            local["w", i, d] = pltpu.make_async_copy(
                weights[i].at[pl.ds(source(d) * chunk, chunk), :], wv.at[i, d], w_sem.at[i, d]
            )
            local["w", i, d].start()
    for h in range(heads):
        local["s", h] = pltpu.make_async_copy(state.at[:, h], sv.at[h], s_sem.at[h])
        local["s", h].start()
    for o in range(tp):
        half = lax.rem(core + o, tp)
        if len(ow.shape) == 3:
            src = ow.at[half]
        else:
            src = ow.at[:, pl.ds(pl.multiple_of(half * cols, 128), cols)]
        local["o", o] = pltpu.make_async_copy(src, owv.at[o], ow_sem.at[o])
        local["o", o].start()

    barrier = pltpu.get_barrier_semaphore()
    group = kv * tp
    flat = me * tp + core

    def peer(o):
        other = lax.rem(flat + o, group)
        return {"kv": other // tp, "tp": lax.rem(other, tp)}

    for o in range(1, group):
        pl.semaphore_signal(barrier, inc=1, device_id=peer(o), device_id_type=MESH_IDS)
    pl.semaphore_wait(barrier, group - 1)

    sent = {}
    for d in range(1, kv):
        sent[d] = pltpu.make_async_remote_copy(
            src_ref=tokens.at[pl.ds(target(d) * rows, rows), :],
            dst_ref=tok.at[d],
            send_sem=tok_send.at[d],
            recv_sem=tok_recv.at[d],
            device_id={"kv": target(d)},
            device_id_type=MESH_IDS,
        )
        sent[d].start()

    squares = jnp.zeros((rows, 1), F32)
    for d in range(kv):
        if d == 0:
            local["tok"].wait()
        else:
            sent[d].wait_recv()
        c = source(d)
        wide = tok[d].astype(F32)
        squares = squares + jnp.sum(wide * wide, axis=1, keepdims=True)
        scaled = (wide * gains[pl.ds(c, 1), :]).astype(BF16)
        small = mm_nt(scaled, bd[:, pl.ds(pl.multiple_of(c * chunk, 128), chunk)])
        if d == 0:
            sacc[...] = small
        else:
            sacc[...] += small
        for i in range(4):
            local["w", i, d].wait()
            y = mm(scaled, wv[i, d])
            if d == 0:
                acc[i] = y
            else:
                acc[i] += y
    for d in range(1, kv):
        sent[d].wait_send()
    inverse = lax.rsqrt(squares / model_width + EPS)

    same, incl, strict = masks_of(rows, proposals)
    raw = sacc[...] * inverse
    rates = 1.0 / (1.0 + jnp.exp(-raw))
    soft = jnp.maximum(raw, 0.0) + jnp.log1p(jnp.exp(-jnp.abs(raw)))
    decays = -jnp.exp(log_row[...]) * soft
    cum = mm_exact(jnp.where(incl, 1.0, 0.0), decays)
    cum_t = cum.T
    moves = {}
    for h in range(heads):
        block = slice(h * size, (h + 1) * size)
        query = unit(silu(acc[0, :, block] * inverse)) * size ** (-0.5)
        key = unit(silu(acc[1, :, block] * inverse))
        value = silu(acc[2, :, block] * inverse)
        gate = silu(acc[3, :, block] * inverse)
        g_col = cum[:, heads + h:heads + h + 1]
        g_row = cum_t[heads + h:heads + h + 1, :]
        pairs = jnp.exp(jnp.where(incl, g_col - g_row, -1e30))
        gamma = jnp.exp(g_col)
        local["s", h].wait()
        recalled, asked = per_sequence(
            [key, query], lambda s, n: sv[h, s:s + n], proposals, rows
        )
        w = solve(key, value, recalled, rates[:, h:h + 1], pairs, gamma, strict)
        mix = (pairs * mm_nt(query.astype(BF16), key.astype(BF16))).astype(BF16)
        reads = gamma * asked + mm(mix, w.astype(BF16))
        normed = reads * lax.rsqrt(jnp.mean(reads * reads, axis=-1, keepdims=True) + EPS)
        att[h] = (normed * head_gain[...] * gate).astype(BF16)
        for d in range(1, kv):
            moves[d, h] = pltpu.make_async_remote_copy(
                src_ref=att.at[h],
                dst_ref=attall.at[d, h],
                send_sem=att_send.at[d, h],
                recv_sem=att_recv.at[d, h],
                device_id={"kv": target(d)},
                device_id_type=MESH_IDS,
            )
            moves[d, h].start()

    for o in range(tp):
        local["o", o].wait()
    swaps = {}
    for d in range(kv):
        for h in range(heads):
            if d:
                moves[d, h].wait_recv()
        if d:
            rows_in = jnp.concatenate([attall[d, h] for h in range(heads)], axis=1)
        else:
            rows_in = jnp.concatenate([att[h] for h in range(heads)], axis=1)
        for o in range(1, tp):
            give[d, o] = mm(rows_in, owv[o]).astype(BF16)
            swaps[d, o] = pltpu.make_async_remote_copy(
                src_ref=give.at[d, o],
                dst_ref=take.at[d, o],
                send_sem=tp_send.at[d, o],
                recv_sem=tp_recv.at[d, o],
                device_id={"tp": lax.rem(core + o, tp)},
                device_id_type=MESH_IDS,
            )
            swaps[d, o].start()
        part[d] = mm(rows_in, owv[0])
    ones = jnp.ones((8, cols), F32)
    for d in range(kv):
        for o in range(1, tp):
            swaps[d, o].wait_recv()
            part[d] += take[d, o].astype(F32)
        mine = part[d]
        line = lax.dot_general(
            ones, mine * mine, (((1,), (1,)), ((), ())),
            preferred_element_type=F32, precision=lax.Precision.HIGHEST,
        )
        sums[pl.ds(source(d), 1), :] = line[0:1]
    tells = {}
    for o in range(1, group):
        tells[o] = pltpu.make_async_remote_copy(
            src_ref=sums,
            dst_ref=sumall.at[o],
            send_sem=sum_send.at[o],
            recv_sem=sum_recv.at[o],
            device_id=peer(o),
            device_id_type=MESH_IDS,
        )
        tells[o].start()
    for key in moves:
        moves[key].wait_send()
    for key in swaps:
        swaps[key].wait_send()
    totals = sums[...]
    for o in range(1, group):
        tells[o].wait_recv()
        totals = totals + sumall[o]
    sums_factor = lax.rsqrt(totals / model_width + EPS)
    for o in range(1, group):
        tells[o].wait_send()
    sums[...] = sums_factor
    for d in range(kv):
        c = source(d)
        factor = jnp.broadcast_to(sums[pl.ds(c, 1), :], (rows, rows)).T[:, 0:1]
        out[pl.ds(pl.multiple_of(c * rows, rows), rows), :] = (
            part[d] * factor * post[...]
        ).astype(BF16)


def make_local(mesh):
    kv = mesh.shape["kv"]
    tp = mesh.shape["tp"]

    def local(
        tokens, pre_gain, query_weight, key_weight, value_weight, gate_weight, beta_weight,
        decay_weight, decay_log, head_gain, out_weight, post_gain, saved_state, earlier_keys,
        earlier_values, earlier_rates, earlier_decays, accepted,
    ):
        seqs, heads, size = saved_state.shape[:3]
        proposals = earlier_keys.shape[1]
        rows = seqs * proposals
        width = heads * size
        model_width = pre_gain.shape[0]
        chunk = tokens.shape[1]
        cols = post_gain.shape[0]
        head_start = lax.axis_index("tp") * heads

        live = (jnp.arange(proposals)[None, :] < accepted[:, None]).astype(F32)[:, :, None]
        bg = jnp.concatenate([earlier_rates * live, earlier_decays * live], axis=2)
        bg = jnp.pad(bg.reshape(rows, 2 * heads), ((0, 0), (0, rows - 2 * heads)))
        state_spec = pl.BlockSpec((seqs, 1, size, size), lambda h: (0, h, 0, 0))
        row_spec = pl.BlockSpec((rows, size), lambda h: (0, h))
        committed = pl.pallas_call(
            functools.partial(commit_kernel, proposals, heads),
            grid=(heads,),
            out_shape=jax.ShapeDtypeStruct(saved_state.shape, F32),
            in_specs=[row_spec, row_spec, pl.BlockSpec((rows, rows), lambda h: (0, 0)), state_spec],
            out_specs=state_spec,
            scratch_shapes=[pltpu.VMEM((rows, rows), F32)] * 3,
            compiler_params=pltpu.CompilerParams(vmem_limit_bytes=VMEM_BYTES),
            cost_estimate=pl.CostEstimate(
                flops=2 * saved_state.size * 2 * proposals,
                bytes_accessed=saved_state.size * 8,
                transcendentals=0,
            ),
            name="commit",
        )(
            earlier_keys.reshape(rows, width),
            earlier_values.reshape(rows, width),
            bg,
            saved_state,
        )

        beta_rows = lax.dynamic_slice_in_dim(beta_weight.T, head_start, heads, 0)
        decay_rows = lax.dynamic_slice_in_dim(decay_weight.T, head_start, heads, 0)
        bd = jnp.pad(
            jnp.concatenate([beta_rows, decay_rows], axis=0), ((0, rows - 2 * heads), (0, 0))
        )
        log_row = jnp.pad(decay_log, (heads, rows - 2 * heads)).reshape(1, rows)
        if cols % 128:
            out_w = jnp.moveaxis(out_weight.reshape(width, tp, cols), 1, 0)
        else:
            out_w = out_weight
        any_spec = pl.BlockSpec(memory_space=pl.ANY)
        vmem_spec = pl.BlockSpec(memory_space=pltpu.VMEM)
        dma = pltpu.SemaphoreType.DMA
        mixed = pl.pallas_call(
            functools.partial(layer_kernel, kv, tp, proposals, heads, model_width),
            out_shape=jax.ShapeDtypeStruct((tokens.shape[0], cols), BF16),
            in_specs=[any_spec, vmem_spec] + [any_spec] * 4 + [vmem_spec] * 3
            + [any_spec, vmem_spec, any_spec],
            out_specs=vmem_spec,
            scratch_shapes=[
                pltpu.VMEM((kv, rows, chunk), BF16),
                pltpu.VMEM((4, kv, chunk, width), BF16),
                pltpu.VMEM((heads, seqs, size, size), F32),
                pltpu.VMEM((tp, width, cols), BF16),
                pltpu.VMEM((4, rows, width), F32),
                pltpu.VMEM((rows, rows), F32),
                pltpu.VMEM((heads, rows, size), BF16),
                pltpu.VMEM((kv, heads, rows, size), BF16),
                pltpu.VMEM((kv, rows, cols), F32),
                pltpu.VMEM((kv, tp, rows, cols), BF16),
                pltpu.VMEM((kv, tp, rows, cols), BF16),
                pltpu.VMEM((kv, rows), F32),
                pltpu.VMEM((kv * tp, kv, rows), F32),
                dma((4, kv)), dma((heads,)), dma((tp,)), dma, dma((kv,)), dma((kv,)),
                dma((kv, heads)), dma((kv, heads)), dma,
                dma((kv, tp)), dma((kv, tp)), dma((kv * tp,)), dma((kv * tp,)),
            ],
            compiler_params=pltpu.CompilerParams(
                collective_id=0, has_side_effects=True, vmem_limit_bytes=VMEM_BYTES
            ),
            name="layer",
        )(
            tokens, pre_gain.reshape(kv, chunk), query_weight, key_weight, value_weight,
            gate_weight, bd, log_row, head_gain.reshape(1, size), out_w,
            post_gain.reshape(1, cols), committed,
        )
        return (mixed, committed)

    return local


def solution(mesh):
    placed = (
        P("dp", "kv"),
        P(),
        P(None, "tp"),
        P(None, "tp"),
        P(None, "tp"),
        P(None, "tp"),
        P(),
        P(),
        P("tp"),
        P(),
        P("tp", "kv"),
        P(("kv", "tp")),
        P(("dp", "kv"), "tp", None, None),
        P(("dp", "kv"), None, "tp", None),
        P(("dp", "kv"), None, "tp", None),
        P(("dp", "kv"), None, "tp"),
        P(("dp", "kv"), None, "tp"),
        P(("dp", "kv")),
    )
    return jax.shard_map(
        make_local(mesh),
        mesh=mesh,
        in_specs=placed,
        out_specs=(P("dp", ("kv", "tp")), P(("dp", "kv"), "tp", None, None)),
        check_vma=False,
    )
```

time: 189 us -> 60.5 us (0.32)
  other arithmetic: 107 us -> 2.24 us
  Pallas kernels: 0 us -> 51.1 us
  blocking collectives: 32.7 us -> 0 us
  between operations: 14.4 us -> 0.66 us
  waiting for transfers between devices: 9.86 us -> 0 us
  matrix products: 6.8 us -> 0 us
  starting transfers between devices: 6.49 us -> 0 us
  local copies, waits for them, and re-layouts: 10.4 us -> 6.13 us
    mul x19 -> x1, other arithmetic: 97.9 us -> 0.72 us  [local(): bg = jnp.concatenate([earlier_rates * live, earlier_decays * live], axis=2)]
    pallas_call x0 -> x2, Pallas kernels: none -> 51.1 us  [the longest x1 41.6 us: local(): pl.pallas_call(functools.partial(layer_kernel, kv, tp, proposals, heads,...]
    psum x1 -> x0, blocking collectives: 17.1 us -> none  [local(): totals = lax.psum(jnp.sum(column_part * column_part, axis=1), ('kv', 'tp'))]
    all_gather x1 -> x0, blocking collectives: 15.7 us -> none  [local(): lax.all_gather(attended, 'kv', axis=0, tiled=True)]
    reduce_scatter x1 -> x0, waiting for transfers between devices: 9.84 us -> none  [local(): lax.psum_scatter(partial_value.astype(jnp.bfloat16), 'tp', scatter_dimens...]
    dot_general x7 -> x0, matrix products: 6.8 us -> none  [the longest x4 5.2 us: local(): jnp.dot(scaled, weight, preferred_element_type=jnp.float32)]
    all_to_all x1 -> x0, starting transfers between devices: 6.49 us -> none  [local(): lax.all_to_all(tokens, 'kv', split_axis=0, concat_axis=1, tiled=True)]
    convert_element_type x6 -> x1, other arithmetic: 6.16 us -> 0.66 us  [local(): (jnp.arange(proposals)[None, :] < accepted[:, None]).astype(F32)[:, :, None]]
  transfers between devices with their start and end apart: 2 -> 0, of which waited for: 1 -> 0; matrix products, arithmetic and copies ran while one was open for 27% -> 0% of each run, Pallas kernels for 0% -> 0%
where the time goes in v1:
time: 60.5 us; the launch traced here: 60.2 us
  Pallas kernels  51.1 us (84%)
  local copies, waits for them, and re-layouts  6.13 us (10%)
  other arithmetic  2.24 us (4%)
  between operations  0.66 us (1%)
    pallas_call x1, Pallas kernels, local(): pl.pallas_call(functools.partial(layer_kernel, kv, tp, proposals, heads,...  41.6 us
    pallas_call x1, Pallas kernels, local(): pl.pallas_call(functools.partial(commit_kernel, proposals, heads), grid=(...  9.5 us
    reshape x1, local copies, waits for them, and re-layouts, local(): earlier_values.reshape(rows, width)  1.69 us
    unnamed x5, local copies, waits for them, and re-layouts  1.68 us

profile of v1, /device:TPU:0, one launch (start us, length us, event | category | flops | bytes accessed | tf_op | source)
XLA Modules:
  0.0 60.2 jit_solution(7390294139099250074)
XLA Ops:
  0.6 0.8 %dynamic-slice_bitcast_fusion = (bf16[4,2048]{1,0:T(4,128)(2,1)S(1)}, bf16[4,2048]{1,0:T(4,128)(2,1)S(1)}) fusion(bf16[2048,8]{0,1:T(8,128)(2,1)} %param.25, s32[]{:T(128)S(6)} %select_n.4, bf16[2048,8]{0,1:T(8,128)(2,1)} %param.24), kind=kLoop, calls=%fused_computation.7 | loop fusion | bytes 65540 | tf_op jit(solution)/shard_map/dynamic_slice | solution.py:359
  1.4 0.9 %fusion.2.bd = bf16[128,2048]{1,0:T(8,128)(2,1)} fusion(bf16[4,2048]{1,0:T(4,128)(2,1)S(1)} %get-tuple-element.4, bf16[4,2048]{1,0:T(4,128)(2,1)S(1)} %get-tuple-element.5), kind=kLoop, calls=%fused_computation.3 | loop fusion | flops 1835008 | bytes 557056 | tf_op jit(solution)/shard_map/concatenate | solution.py:361
  2.3 0.7 %fusion.3 = f32[32,4]{0,1:T(4,128)S(1)} fusion(s32[32]{0:T(128)} %param.35), kind=kLoop, calls=%fused_computation.12 | loop fusion | flops 256 | bytes 640 | tf_op jit(solution)/shard_map/convert_element_type | solution.py:332
  2.9 0.7 %broadcast_multiply_fusion.1 = (f32[32,4,4]{0,2,1:T(4,128)S(1)}, f32[32,4,4]{0,2,1:T(4,128)S(1)}) fusion(f32[32,4,4]{0,2,1:T(4,128)} %param.33, f32[32,4]{0,1:T(4,128)S(1)} %fusion.3, f32[32,4,4]{0,2,1:T(4,128)} %param.34), kind=kLoop, calls=%fused_computation.10 | loop fusion | flops 1024 | bytes 8704 | tf_op jit(solution)/shard_map/mul | solution.py:333
  3.7 0.1 copy.20
  3.8 0.6 %pad.14.bg_ref = f32[128,128]{1,0:T(8,128)} pad(f32[128,8]{1,0:T(8,128)S(1)} %bitcast.17, f32[]{:T(128)} %constant.13.clone.1), padding=0_0x0_120 | pad | bytes 69636 | tf_op jit(solution)/shard_map/jit(_pad)/pad | solution.py:334
  4.4 1.7 %copy_bitcast_fusion = (bf16[128,512]{1,0:T(8,128)(2,1)}, bf16[128,512]{1,0:T(8,128)(2,1)}) fusion(bf16[16,8,4,128]{3,2,1,0:T(4,128)(2,1)} %bitcast.18, bf16[16,8,4,128]{3,2,1,0:T(4,128)(2,1)} %bitcast.19), kind=kLoop, calls=%fused_computation.4 | loop fusion | bytes 524288 | tf_op jit(solution)/shard_map/reshape | solution.py:353
  6.1 0.0 copy-start
  6.1 0.0 copy-start.1
  6.1 9.5 %commit.1.state = f32[32,4,128,128]{3,2,1,0:T(8,128)} custom-call(bf16[128,512]{1,0:T(8,128)(2,1)} %get-tuple-element.7.keys_ref, bf16[128,512]{1,0:T(8,128)(2,1)} %get-tuple-element.6.values_ref, f32[128,128]{1,0:T(8,128)} %pad.14.bg_ref, f32[32,4,128,128]{3,2,1,0:T(8,128)} %state_ref.1), custom_call_target="tpu_custom_call" | custom-call | flops 33554432 | bytes 16777216 | tf_op jit(solution)/shard_map/commit/pallas_call | solution.py:337
  15.6 0.0 copy-done
  15.6 0.6 %reshape.47.gains = f32[4,512]{1,0:T(4,128)} reshape(f32[2048]{0:T(1024)S(1)} %copy-done) | data formatting | bytes 16384 | tf_op jit(solution)/shard_map/reshape | solution.py:400
  16.2 0.0 copy-done.1
  16.2 0.6 %pad_bitcast_fusion.log_row = f32[1,128]{1,0:T(1,128)} fusion(f32[4]{0:T(128)S(1)} %copy-done.1), kind=kLoop, calls=%fused_computation.13 | loop fusion | bytes 528 | tf_op jit(solution)/shard_map/reshape | solution.py:363
  16.8 41.6 %layer.1 = bf16[512,256]{1,0:T(8,128)(2,1)} custom-call(bf16[512,512]{1,0:T(8,128)(2,1)} %tokens.1, f32[4,512]{1,0:T(4,128)} %reshape.47.gains, bf16[2048,512]{1,0:T(8,128)(2,1)} %qw.1, bf16[2048,512]{1,0:T(8,128)(2,1)} %kw.1, bf16[2048,512]{1,0:T(8,128)(2,1)} %vw.1, bf16[2048,512]{1,0:T(8,128)(2,1)} %gw.1, bf16[128,2048]{1,0:T(8,128)(2,1)} %fusion.2.bd, ...), custom_call_target="tpu_custom_call" | custom-call | tf_op jit(solution)/shard_map/layer/pallas_call | solution.py:371
  58.5 1.7 %copy.26 = bf16[512,256]{1,0:T(8,128)(2,1)} copy(bf16[512,256]{1,0:T(8,128)(2,1)} %layer.1) | data formatting | bytes 524288
  (1 shorter events, 0.0 us)
Async XLA Ops:
  6.1 9.5 %copy-start = (f32[2048]{0:T(1024)S(1)}, f32[2048]{0:T(1024)}, u32[]{:S(2)}) copy-start(f32[2048]{0:T(1024)} %param.19) | copy-start | bytes 24580
  6.1 10.1 %copy-start.1 = (f32[4]{0:T(128)S(1)}, f32[4]{0:T(128)}, u32[]{:S(2)}) copy-start(f32[4]{0:T(128)} %param.26) | copy-start | bytes 52

commit v2 on v1

v2 whole, which is shorter than its diff:
```python
import functools

import jax
import jax.numpy as jnp
from jax import lax
from jax.experimental import pallas as pl
from jax.experimental.pallas import tpu as pltpu
from jax.sharding import PartitionSpec as P

F32 = jnp.float32
BF16 = jnp.bfloat16
EPS = 1e-06
MESH_IDS = pl.DeviceIdType.MESH
VMEM_BYTES = 60 * 1024 * 1024


def mm(a, b):
    return jnp.dot(a, b, preferred_element_type=F32)


def mm_nt(a, b):
    return lax.dot_general(a, b, (((1,), (1,)), ((), ())), preferred_element_type=F32)


def mm_tn(a, b):
    return lax.dot_general(a, b, (((0,), (0,)), ((), ())), preferred_element_type=F32)


def mm_exact(a, b):
    return jnp.dot(a, b, preferred_element_type=F32, precision=lax.Precision.HIGHEST)


def unit(values):
    return values * lax.rsqrt(jnp.sum(values * values, axis=-1, keepdims=True) + EPS)


def silu(values):
    return values / (1.0 + jnp.exp(-values))


def masks_of(rows, proposals):
    r = lax.broadcasted_iota(jnp.int32, (rows, rows), 0)
    c = lax.broadcasted_iota(jnp.int32, (rows, rows), 1)
    same = (r // proposals) == (c // proposals)
    return same, same & (c <= r), same & (c < r)


def per_sequence(operands, state_of, proposals, rows):
    size = operands[0].shape[1]
    group = 16
    seqs = group // proposals
    stack = group * len(operands)
    row = lax.broadcasted_iota(jnp.int32, (stack, size), 0)
    owner = (row % group) // proposals
    outs = [[] for _ in operands]
    for g in range(rows // group):
        x = jnp.concatenate([o[g * group:(g + 1) * group] for o in operands], axis=0)
        lhs = jnp.concatenate(
            [jnp.where(owner == s, x, 0.0).astype(BF16) for s in range(seqs)], axis=1
        )
        rhs = state_of(g * seqs, seqs).reshape(seqs * size, size).astype(BF16)
        y = mm(lhs, rhs)
        for i in range(len(operands)):
            outs[i].append(y[i * group:(i + 1) * group])
    return [jnp.concatenate(o, axis=0) for o in outs]


def solve(keys, values, recalled, rate, decay_pairs, gamma, strict):
    kb = keys.astype(BF16)
    low = (jnp.where(strict, decay_pairs * mm_nt(kb, kb), 0.0) * rate).astype(BF16)
    rhs = rate * (values - gamma * recalled)
    square = mm(low, low).astype(BF16)
    x = rhs + mm(square, rhs.astype(BF16))
    return x - mm(low, x.astype(BF16))


def commit_kernel(proposals, keys_ref, values_ref, rates_ref, decays_ref, accepted_ref, state_ref, out_ref):
    h = pl.program_id(0)
    rows, size = keys_ref.shape
    seqs = accepted_ref.shape[1]
    same, incl, strict = masks_of(rows, proposals)
    row = lax.broadcasted_iota(jnp.int32, (rows, seqs), 0)
    own = (row // proposals) == lax.broadcasted_iota(jnp.int32, (rows, seqs), 1)

    def line(ref, p):
        return jnp.where(accepted_ref[...] > p, ref[p, pl.ds(h, 1), :], 0.0)

    def column(lines):
        spread = jnp.zeros((rows, seqs), F32)
        for p in range(proposals):
            spread = jnp.where(own & (row % proposals == p), lines[p], spread)
        return jnp.sum(spread, axis=1, keepdims=True)

    rate = column([line(rates_ref, p) for p in range(proposals)])
    sums = [line(decays_ref, 0)]
    for p in range(1, proposals):
        sums.append(sums[-1] + line(decays_ref, p))
    g_col = column(sums)
    g_last = column([sums[-1]] * proposals)
    g_row = jnp.broadcast_to(g_col, (rows, rows)).T
    pairs = jnp.exp(jnp.where(incl, g_col - g_row, -1e30))
    keys = unit(keys_ref[...].astype(F32))
    (recalled,) = per_sequence(
        [keys], lambda s, n: state_ref[s:s + n, 0], proposals, rows
    )
    w = solve(keys, values_ref[...].astype(F32), recalled, rate, pairs, jnp.exp(g_col), strict)
    scaled_keys = (keys * jnp.exp(g_last - g_col)).astype(BF16)
    whole = jnp.broadcast_to(jnp.exp(g_last), (rows, size))
    group = 16
    seqs = group // proposals
    owner = lax.broadcasted_iota(jnp.int32, (group, size), 0) // proposals
    for g in range(rows // group):
        wg = w[g * group:(g + 1) * group]
        spread = jnp.concatenate(
            [jnp.where(owner == s, wg, 0.0).astype(BF16) for s in range(seqs)], axis=1
        )
        add = mm_tn(scaled_keys[g * group:(g + 1) * group], spread)
        for s in range(seqs):
            seq = g * seqs + s
            keep = whole[seq * proposals:seq * proposals + 1]
            out_ref[seq, 0] = keep * state_ref[seq, 0] + add[:, s * size:(s + 1) * size]


def layer_kernel(
    kv, tp, proposals, heads, model_width,
    tokens, gains, qw, kw, vw, gw, beta_t, decay_t, log_rate, head_gain, ow, post, state,
    out,
    tok, wv, sv, owv, acc, bacc, dacc, att, passed, part, give, take, sums, sumall,
    w_sem, s_sem, ow_sem, own_sem, tok_send, tok_recv, half_send, half_recv, att_send, att_recv,
    tp_send, tp_recv, sum_send, sum_recv,
):
    me = lax.axis_index("kv")
    core = lax.axis_index("tp")
    rows, chunk = tok.shape[1], tok.shape[2]
    size = head_gain.shape[1]
    cols = out.shape[1]
    weights = (qw, kw, vw, gw)

    def source(d):
        return lax.rem(me - d + kv, kv)

    def target(d):
        return lax.rem(me + d, kv)

    local = {}
    local["tok"] = pltpu.make_async_copy(tokens.at[pl.ds(me * rows, rows), :], tok.at[0], own_sem)
    local["tok"].start()
    for d in range(kv):
        for i in range(4):
            local["w", i, d] = pltpu.make_async_copy(
                weights[i].at[pl.ds(source(d) * chunk, chunk), :], wv.at[i, d], w_sem.at[i, d]
            )
            local["w", i, d].start()
    for h in range(heads):
        local["s", h] = pltpu.make_async_copy(state.at[:, h], sv.at[h], s_sem.at[h])
        local["s", h].start()
    for o in range(tp):
        half = lax.rem(core + o, tp)
        if len(ow.shape) == 3:
            src = ow.at[half]
        else:
            src = ow.at[:, pl.ds(pl.multiple_of(half * cols, 128), cols)]
        local["o", o] = pltpu.make_async_copy(src, owv.at[o], ow_sem.at[o])
        local["o", o].start()

    barrier = pltpu.get_barrier_semaphore()
    group = kv * tp
    flat = me * tp + core

    def peer(o):
        other = lax.rem(flat + o, group)
        return {"kv": other // tp, "tp": lax.rem(other, tp)}

    for o in range(1, group):
        pl.semaphore_signal(barrier, inc=1, device_id=peer(o), device_id_type=MESH_IDS)
    pl.semaphore_wait(barrier, group - 1)

    part_rows = rows // tp
    mine_rows = pl.ds(pl.multiple_of(core * part_rows, part_rows), part_rows)
    sent = {}
    halves = {}
    for d in range(1, kv):
        sent[d] = pltpu.make_async_remote_copy(
            src_ref=tokens.at[
                pl.ds(pl.multiple_of(target(d) * rows + core * part_rows, part_rows), part_rows), :
            ],
            dst_ref=tok.at[d, mine_rows],
            send_sem=tok_send.at[d],
            recv_sem=tok_recv.at[d],
            device_id={"kv": target(d)},
            device_id_type=MESH_IDS,
        )
        sent[d].start()

    def hand_over(d):
        sent[d].wait_recv()
        for o in range(1, tp):
            halves[d, o] = pltpu.make_async_remote_copy(
                src_ref=tok.at[d, mine_rows],
                dst_ref=tok.at[d, mine_rows],
                send_sem=half_send.at[d, o],
                recv_sem=half_recv.at[d, o],
                device_id={"tp": lax.rem(core + o, tp)},
                device_id_type=MESH_IDS,
            )
            halves[d, o].start()

    def project(d, squares):
        if d == 0:
            local["tok"].wait()
        else:
            for o in range(1, tp):
                halves[d, o].wait_recv()
        c = source(d)
        span = pl.ds(pl.multiple_of(c * chunk, 128), chunk)
        wide = tok[d].astype(F32)
        scaled = (wide * gains[:, span]).astype(BF16)
        small_b = mm_nt(scaled, beta_t[:, span])
        small_d = mm_nt(scaled, decay_t[:, span])
        if d == 0:
            bacc[...] = small_b
            dacc[...] = small_d
        else:
            bacc[...] += small_b
            dacc[...] += small_d
        for i in range(4):
            local["w", i, d].wait()
            y = mm(scaled, wv[i, d])
            if d == 0:
                acc[i] = y
            else:
                acc[i] += y
        return squares + jnp.sum(wide * wide, axis=1, keepdims=True)

    squares = project(0, jnp.zeros((rows, 1), F32))
    for d in range(1, kv):
        hand_over(d)
        if d > 1:
            squares = project(d - 1, squares)
    if kv > 1:
        squares = project(kv - 1, squares)
    inverse = lax.rsqrt(squares / model_width + EPS)

    same, incl, strict = masks_of(rows, proposals)
    head_lane = lax.broadcasted_iota(jnp.int32, bacc.shape, 1)

    def column(values, h):
        return jnp.sum(jnp.where(head_lane == core * heads + h, values, 0.0), axis=1, keepdims=True)

    rates = 1.0 / (1.0 + jnp.exp(-bacc[...] * inverse))
    raw = dacc[...] * inverse
    soft = jnp.maximum(raw, 0.0) + jnp.log1p(jnp.exp(-jnp.abs(raw)))
    lane = lax.broadcasted_iota(jnp.int32, (rows, rows), 1)
    decays = jnp.zeros((rows, rows), F32)
    for h in range(heads):
        decay = -jnp.exp(jnp.full((rows, 1), log_rate[h], F32)) * column(soft, h)
        decays = jnp.where(lane == h, decay, decays)
    cum = mm_exact(jnp.where(incl, 1.0, 0.0), decays)
    cum_t = cum.T

    def hop(way, s, h):
        step = 1 if way == 0 else kv - 1
        return pltpu.make_async_remote_copy(
            src_ref=att.at[h] if s == 0 else passed.at[way, s, h],
            dst_ref=passed.at[way, s + 1, h],
            send_sem=att_send.at[way, s, h],
            recv_sem=att_recv.at[way, s + 1, h],
            device_id={"kv": lax.rem(me + step, kv)},
            device_id_type=MESH_IDS,
        )

    def arrives(way, s):
        return me - s >= 0 if way == 0 else me + s < kv

    def leaves(way):
        return me + 1 < kv if way == 0 else me >= 1

    def advance(turn):
        for s in range(kv):
            h = turn - s
            if not 0 <= h < heads:
                continue
            for way in range(2):
                if s == 0:
                    @pl.when(leaves(way))
                    def _():
                        hop(way, 0, h).start()
                else:
                    @pl.when(arrives(way, s))
                    def _():
                        hop(way, s - 1, h).wait_recv()
                    if s < kv - 1:
                        @pl.when(arrives(way, s) & leaves(way))
                        def _():
                            hop(way, s, h).start()

    def settle():
        for s in range(kv - 1):
            for way in range(2):
                @pl.when(arrives(way, s) & leaves(way))
                def _():
                    for h in range(heads):
                        hop(way, s, h).wait_send()

    for first in range(heads):
        batch = range(first, first + 1)
        local["s", first].wait()
        query, key, pairs, gamma, w, asked, reads = {}, {}, {}, {}, {}, {}, {}
        recalled = {}
        for h in batch:
            block = slice(h * size, (h + 1) * size)
            query[h] = unit(silu(acc[0, :, block] * inverse)) * size ** (-0.5)
            key[h] = unit(silu(acc[1, :, block] * inverse))
            pairs[h] = jnp.exp(jnp.where(incl, cum[:, h:h + 1] - cum_t[h:h + 1, :], -1e30))
            gamma[h] = jnp.exp(cum[:, h:h + 1])
        for h in batch:
            recalled[h], asked[h] = per_sequence(
                [key[h], query[h]], lambda s, n, h=h: sv[h, s:s + n], proposals, rows
            )
        for h in batch:
            value = silu(acc[2, :, h * size:(h + 1) * size] * inverse)
            w[h] = solve(key[h], value, recalled[h], column(rates, h), pairs[h], gamma[h], strict)
        for h in batch:
            mix = (pairs[h] * mm_nt(query[h].astype(BF16), key[h].astype(BF16))).astype(BF16)
            reads[h] = gamma[h] * asked[h] + mm(mix, w[h].astype(BF16))
        for h in batch:
            gate = silu(acc[3, :, h * size:(h + 1) * size] * inverse)
            scale = lax.rsqrt(jnp.mean(reads[h] * reads[h], axis=-1, keepdims=True) + EPS)
            att[h] = (reads[h] * scale * head_gain[...] * gate).astype(BF16)
        for h in batch:
            advance(h)

    for o in range(tp):
        local["o", o].wait()

    def swap(c, o):
        return pltpu.make_async_remote_copy(
            src_ref=give.at[c, o],
            dst_ref=take.at[c, o],
            send_sem=tp_send.at[c, o],
            recv_sem=tp_recv.at[c, o],
            device_id={"tp": lax.rem(core + o, tp)},
            device_id_type=MESH_IDS,
        )

    def combine(c, pieces):
        rows_in = jnp.concatenate(pieces, axis=1)
        for o in range(1, tp):
            give[c, o] = mm(rows_in, owv[o]).astype(BF16)
            swap(c, o).start()
        part[c] = mm(rows_in, owv[0])

    def finish(c):
        own = part[c]
        for o in range(1, tp):
            swap(c, o).wait_recv()
            own = own + take[c, o].astype(F32)
        part[c] = own
        total = jnp.sum(own * own, axis=1, keepdims=True)
        sums[pl.ds(c, 1), :] = jnp.broadcast_to(total, (rows, rows)).T[0:1]

    def blocks(turn):
        if turn < heads:
            return [(True, me, None)]
        s = turn - heads + 1
        return [(arrives(way, s), me - s if way == 0 else me + s, way) for way in range(2)]

    combine(me, [att[h] for h in range(heads)])
    for turn in range(heads, heads + kv - 1):
        advance(turn)
        s = turn - heads + 1
        for here, c, way in blocks(turn):
            @pl.when(here)
            def _():
                combine(c, [passed[way, s, h] for h in range(heads)])
        if s == 1:
            finish(me)
        else:
            for here, c, way in blocks(turn - 1):
                @pl.when(here)
                def _():
                    finish(c)
    if kv > 1:
        for here, c, way in blocks(heads + kv - 2):
            @pl.when(here)
            def _():
                finish(c)
    else:
        finish(me)
    tells = {}
    for o in range(1, group):
        tells[o] = pltpu.make_async_remote_copy(
            src_ref=sums,
            dst_ref=sumall.at[o],
            send_sem=sum_send.at[o],
            recv_sem=sum_recv.at[o],
            device_id=peer(o),
            device_id_type=MESH_IDS,
        )
        tells[o].start()
    settle()
    for d in range(1, kv):
        sent[d].wait_send()
        for o in range(1, tp):
            halves[d, o].wait_send()
    for c in range(kv):
        for o in range(1, tp):
            swap(c, o).wait_send()
    totals = sums[...]
    for o in range(1, group):
        tells[o].wait_recv()
        totals = totals + sumall[o]
    sums_factor = lax.rsqrt(totals / model_width + EPS)
    for o in range(1, group):
        tells[o].wait_send()
    for c in range(kv):
        factor = jnp.broadcast_to(sums_factor[c:c + 1, :], (rows, rows)).T[:, 0:1]
        out[c * rows:(c + 1) * rows, :] = (part[c] * factor * post[...]).astype(BF16)


def make_local(mesh):
    kv = mesh.shape["kv"]
    tp = mesh.shape["tp"]

    def local(
        tokens, pre_gain, query_weight, key_weight, value_weight, gate_weight, beta_weight,
        decay_weight, decay_log, head_gain, out_weight, post_gain, saved_state, earlier_keys,
        earlier_values, earlier_rates, earlier_decays, accepted,
    ):
        seqs, heads, size = saved_state.shape[:3]
        proposals = earlier_keys.shape[1]
        rows = seqs * proposals
        width = heads * size
        model_width = pre_gain.shape[0]
        chunk = tokens.shape[1]
        cols = post_gain.shape[0]
        state_spec = pl.BlockSpec((seqs, 1, size, size), lambda h: (0, h, 0, 0))
        row_spec = pl.BlockSpec((rows, size), lambda h: (0, h))
        scalar_spec = pl.BlockSpec((proposals, heads, seqs), lambda h: (0, 0, 0))
        committed = pl.pallas_call(
            functools.partial(commit_kernel, proposals),
            grid=(heads,),
            out_shape=jax.ShapeDtypeStruct(saved_state.shape, F32),
            in_specs=[
                row_spec, row_spec, scalar_spec, scalar_spec,
                pl.BlockSpec((1, seqs), lambda h: (0, 0)), state_spec,
            ],
            out_specs=state_spec,
            compiler_params=pltpu.CompilerParams(vmem_limit_bytes=VMEM_BYTES),
            cost_estimate=pl.CostEstimate(
                flops=2 * saved_state.size * 2 * proposals,
                bytes_accessed=saved_state.size * 8,
                transcendentals=0,
            ),
            name="commit",
        )(
            earlier_keys.reshape(rows, width),
            earlier_values.reshape(rows, width),
            jnp.transpose(earlier_rates, (1, 2, 0)),
            jnp.transpose(earlier_decays, (1, 2, 0)),
            accepted.reshape(1, seqs),
            saved_state,
        )

        if cols % 128:
            out_w = jnp.moveaxis(out_weight.reshape(width, tp, cols), 1, 0)
        else:
            out_w = out_weight
        any_spec = pl.BlockSpec(memory_space=pl.ANY)
        vmem_spec = pl.BlockSpec(memory_space=pltpu.VMEM)
        dma = pltpu.SemaphoreType.DMA
        mixed = pl.pallas_call(
            functools.partial(layer_kernel, kv, tp, proposals, heads, model_width),
            out_shape=jax.ShapeDtypeStruct((tokens.shape[0], cols), BF16),
            in_specs=[any_spec, vmem_spec] + [any_spec] * 4 + [vmem_spec] * 2
            + [pl.BlockSpec(memory_space=pltpu.SMEM), vmem_spec, any_spec, vmem_spec, any_spec],
            out_specs=vmem_spec,
            scratch_shapes=[
                pltpu.VMEM((kv, rows, chunk), BF16),
                pltpu.VMEM((4, kv, chunk, width), BF16),
                pltpu.VMEM((heads, seqs, size, size), F32),
                pltpu.VMEM((tp, width, cols), BF16),
                pltpu.VMEM((4, rows, width), F32),
                pltpu.VMEM((rows, heads * tp), F32),
                pltpu.VMEM((rows, heads * tp), F32),
                pltpu.VMEM((heads, rows, size), BF16),
                pltpu.VMEM((2, kv, heads, rows, size), BF16),
                pltpu.VMEM((kv, rows, cols), F32),
                pltpu.VMEM((kv, tp, rows, cols), BF16),
                pltpu.VMEM((kv, tp, rows, cols), BF16),
                pltpu.VMEM((kv, rows), F32),
                pltpu.VMEM((kv * tp, kv, rows), F32),
                dma((4, kv)), dma((heads,)), dma((tp,)), dma, dma((kv,)), dma((kv,)),
                dma((kv, tp)), dma((kv, tp)), dma((2, kv, heads)), dma((2, kv, heads)),
                dma((kv, tp)), dma((kv, tp)), dma((kv * tp,)), dma((kv * tp,)),
            ],
            compiler_params=pltpu.CompilerParams(
                collective_id=0, has_side_effects=True, vmem_limit_bytes=VMEM_BYTES
            ),
            name="layer",
        )(
            tokens, pre_gain.reshape(1, model_width), query_weight, key_weight, value_weight,
            gate_weight, beta_weight.T, decay_weight.T, decay_log, head_gain.reshape(1, size), out_w,
            post_gain.reshape(1, cols), committed,
        )
        return (mixed, committed)

    return local


def solution(mesh):
    placed = (
        P("dp", "kv"),
        P(),
        P(None, "tp"),
        P(None, "tp"),
        P(None, "tp"),
        P(None, "tp"),
        P(),
        P(),
        P("tp"),
        P(),
        P("tp", "kv"),
        P(("kv", "tp")),
        P(("dp", "kv"), "tp", None, None),
        P(("dp", "kv"), None, "tp", None),
        P(("dp", "kv"), None, "tp", None),
        P(("dp", "kv"), None, "tp"),
        P(("dp", "kv"), None, "tp"),
        P(("dp", "kv")),
    )
    return jax.shard_map(
        make_local(mesh),
        mesh=mesh,
        in_specs=placed,
        out_specs=(P("dp", ("kv", "tp")), P(("dp", "kv"), "tp", None, None)),
        check_vma=False,
    )
```

time: 60.5 us -> 52.3 us (0.86)
  Pallas kernels: 51.1 us -> 48 us
  local copies, waits for them, and re-layouts: 6.13 us -> 3.36 us
  other arithmetic: 2.24 us -> 0 us
    pallas_call x1, Pallas kernels: 41.6 us -> 38.6 us  [local(): pl.pallas_call(functools.partial(layer_kernel, kv, tp, proposals, heads,...]
    reshape x2 -> x0, local copies, waits for them, and re-layouts: 1.24 us -> none  [the longest x1 0.64 us: local(): log_row = jnp.pad(decay_log, (heads, rows - 2 * heads)).reshape(1, rows)]
    concatenate x2 -> x0, other arithmetic: 0.86 us -> none  [the longest x1 0.85 us: local(): jnp.concatenate([beta_rows, decay_rows], axis=0)]
    dynamic_slice x1 -> x0, local copies, waits for them, and re-layouts: 0.8 us -> none  [local(): decay_rows = lax.dynamic_slice_in_dim(decay_weight.T, head_start, heads, 0)]
    mul x1 -> x0, other arithmetic: 0.72 us -> none  [local(): bg = jnp.concatenate([earlier_rates * live, earlier_decays * live], axis=2)]
    convert_element_type x1 -> x0, other arithmetic: 0.66 us -> none  [local(): (jnp.arange(proposals)[None, :] < accepted[:, None]).astype(F32)[:, :, None]]
    pad x1 -> x0, local copies, waits for them, and re-layouts: 0.64 us -> none  [local(): bg = jnp.pad(bg.reshape(rows, 2 * heads), ((0, 0), (0, rows - 2 * heads)))]
    unnamed x5 -> x1, local copies, waits for them, and re-layouts: 1.68 us -> 1.67 us
where the time goes in v2:
time: 52.3 us; the launch traced here: 52 us
  Pallas kernels  48 us (92%)
  local copies, waits for them, and re-layouts  3.36 us (6%)
  between operations  0.64 us (1%)
    pallas_call x1, Pallas kernels, local(): pl.pallas_call(functools.partial(layer_kernel, kv, tp, proposals, heads,...  38.6 us
    pallas_call x1, Pallas kernels, local(): pl.pallas_call(functools.partial(commit_kernel, proposals), grid=(heads,)...  9.46 us
    reshape x1, local copies, waits for them, and re-layouts, local(): earlier_values.reshape(rows, width)  1.69 us
    unnamed x1, local copies, waits for them, and re-layouts  1.67 us

profile of v2, /device:TPU:0, one launch (start us, length us, event | category | flops | bytes accessed | tf_op | source)
XLA Modules:
  0.0 52.0 jit_solution(7719303605251391067)
XLA Ops:
  0.6 1.7 %copy_bitcast_fusion = (bf16[128,512]{1,0:T(8,128)(2,1)}, bf16[128,512]{1,0:T(8,128)(2,1)}) fusion(bf16[16,8,4,128]{3,2,1,0:T(4,128)(2,1)} %bitcast.16, bf16[16,8,4,128]{3,2,1,0:T(4,128)(2,1)} %bitcast.17), kind=kLoop, calls=%fused_computation | loop fusion | bytes 524288 | tf_op jit(solution)/shard_map/reshape | solution.py:458
  2.3 9.5 %commit.1.state = f32[32,4,128,128]{3,2,1,0:T(8,128)} custom-call(bf16[128,512]{1,0:T(8,128)(2,1)} %get-tuple-element.3.keys_ref, bf16[128,512]{1,0:T(8,128)(2,1)} %get-tuple-element.2.values_ref, f32[4,4,32]{2,1,0:T(4,128)} %bitcast.20, f32[4,4,32]{2,1,0:T(4,128)} %bitcast.21, s32[1,32]{1,0:T(1,128)} %bitcast.24, f32[32,4,128,128]{3,2,1,0:T(8,128)} %state_ref.1), custom_call_target="tpu_custom_call" | custom-call | flops 33554432 | bytes 16777216 | tf_op jit(solution)/shard_map/commit/pallas_call | solution.py:440
  11.8 38.6 %layer.1 = bf16[512,256]{1,0:T(8,128)(2,1)} custom-call(bf16[512,512]{1,0:T(8,128)(2,1)} %tokens.1, f32[1,2048]{1,0:T(1,128)} %bitcast.22, bf16[2048,512]{1,0:T(8,128)(2,1)} %qw.1, bf16[2048,512]{1,0:T(8,128)(2,1)} %kw.1, bf16[2048,512]{1,0:T(8,128)(2,1)} %vw.1, bf16[2048,512]{1,0:T(8,128)(2,1)} %gw.1, bf16[8,2048]{1,0:T(8,128)(2,1)} %bitcast.18, ...), custom_call_target="tpu_custom_call" | custom-call | tf_op jit(solution)/shard_map/layer/pallas_call | solution.py:472
  50.4 1.7 %copy.25 = bf16[512,256]{1,0:T(8,128)(2,1)} copy(bf16[512,256]{1,0:T(8,128)(2,1)} %layer.1) | data formatting | bytes 524288
